TPU v7x, 32 devices: a whole 2x2x4 slice. The times are simulated.
32 devices in a mesh: grp: 2 (over x), ep: 16 (over z, y, core).
Axes of the slice: x: 2, y: 2, z: 4, core: 2. Of those that a mesh axis runs over, the one named last changes fastest.
Arguments:
- residual: bfloat16 [16, 4096], P('grp', 'ep'), parts along dimension 0, may hold values from -6 to 6
- head_states: float32 [64, 512, 1024], P(('grp', 'ep')), parts along dimension 0, may hold values from -6 to 6
- first_gain: bfloat16 [4096], replicated, may hold values from 0.099609375 to 1.8984375
- w_query: bfloat16 [4096, 2048], P(None, 'ep'), may hold values from -0.09375 to 0.09375
- w_key: bfloat16 [4096, 2048], P(None, 'ep'), may hold values from -0.09375 to 0.09375
- w_value: bfloat16 [4096, 4096], P(None, 'ep'), may hold values from -0.09375 to 0.09375
- w_gate: bfloat16 [4096, 4096], P(None, 'ep'), may hold values from -0.09375 to 0.09375
- w_low: bfloat16 [4096, 16], replicated, may hold values from -0.09375 to 0.09375
- w_decay: bfloat16 [16, 2048], replicated, may hold values from -15 to 15
- decay_bias: float32 [2048], replicated, may hold values from -40 to 4
- head_gain: bfloat16 [1024], replicated, may hold values from 0.099609375 to 1.8984375
- w_output: bfloat16 [4096, 4096], P(None, 'ep'), may hold values from -0.09375 to 0.09375
- second_gain: bfloat16 [4096], replicated, may hold values from 0.099609375 to 1.8984375
- routes: int32 [16, 2], P('grp'), parts along dimension 0, may hold values from 0 to 15, as said below
- group_logits: float32 [16, 4], P('grp'), parts along dimension 0, may hold values from -12 to 12
- expert_logits: float32 [16, 2], P('grp'), parts along dimension 0, may hold values from -9 to 9
- expert_gate: bfloat16 [16, 4096, 512], P('ep'), may hold values from -0.09375 to 0.09375
- expert_up: bfloat16 [16, 4096, 512], P('ep'), may hold values from -0.09375 to 0.09375
- expert_down: bfloat16 [16, 512, 4096], P('ep'), may hold values from -0.25 to 0.25
Outputs:
- layer_out: bfloat16 [16, 4096], P('grp', 'ep'), parts along dimension 0
- new_states: float32 [64, 512, 1024], P(('grp', 'ep')), parts along dimension 0
There are 2 independent parts, one for each index of `grp`. A program takes and returns all parts, laid end to end along the dimension named above; an argument that names none is the same for every part. Nothing has to cross between parts.
Inputs may be any that keep to these rules, and one draw needn't show every extreme that they name: `routes`: each row names 2 different experts of one group (numbers g * 4 to g * 4 + 3). No expert is named by more than 2 rows, and in every draw all experts of one group are named by exactly 2 rows.
All inputs are finite; a program needn't handle non-finite values.
Results may differ from a plain program's by a relative error of at most 0.014.
Values may be sent and summed in bfloat16 or wider, within the bound.
No kernel may reach another device: no remote copies, remote signals or barrier semaphores. Data moves between devices by JAX's collectives and lax.ppermute only.
A program may use at most 128 MiB of HBM per device.

v0:
```python
import jax
import jax.numpy as jnp
import numpy as np
from jax import lax
from jax.sharding import PartitionSpec as P

HEADS = 4
DK = 512
DV = 1024
GROUPS = 4
TOP = 2


norm_eps = 1e-06
decay_tau = 16.0


def rms_scale(values, gain):
    floats = values.astype(jnp.float32)
    return (
        floats
        * lax.rsqrt(jnp.mean(floats * floats, axis=-1, keepdims=True) + norm_eps)
        * gain.astype(jnp.float32)
    )


def route_weights(routes, group_logits, expert_logits, per_group):
    group_exp = jnp.exp(group_logits)
    group_prob = group_exp / jnp.sum(group_exp, axis=1, keepdims=True)
    chosen = routes[:, 0] // per_group
    groups_row = jnp.arange(group_logits.shape[1], dtype=jnp.int32)
    picked = jnp.sum(
        group_prob * (chosen[:, None] == groups_row[None, :]).astype(jnp.float32), axis=1
    )
    expert_exp = jnp.exp(expert_logits)
    return expert_exp / jnp.sum(expert_exp, axis=1, keepdims=True) * picked[:, None]


def per_device(
    residual,
    head_states,
    first_gain,
    w_query,
    w_key,
    w_value,
    w_gate,
    w_low,
    w_decay,
    decay_bias,
    head_gain,
    w_output,
    second_gain,
    routes,
    group_logits,
    expert_logits,
    expert_gate,
    expert_up,
    expert_down,
):
    devices = lax.axis_size("ep")
    my_index = lax.axis_index("ep")
    seq_count = residual.shape[0]
    own_width = residual.shape[1]
    width = own_width * devices
    pairs_dev = head_states.shape[0]
    slot_count = max(1, pairs_dev // HEADS)
    rows = lax.all_gather(residual, "ep", axis=1, tiled=True)
    normed = rms_scale(rows, first_gain).astype(jnp.bfloat16)
    my_head = my_index * HEADS // devices
    target = jnp.arange(devices, dtype=jnp.int32)[:, None]
    turn = jnp.arange(slot_count, dtype=jnp.int32)[None, :]
    within = jnp.mod(my_head - target * pairs_dev, HEADS) + turn * HEADS
    target_seq = (target * pairs_dev + within) // HEADS
    seq_row = jnp.arange(seq_count, dtype=jnp.int32)[None, None, :]
    picker = (target_seq[:, :, None] == seq_row) & (within < pairs_dev)[:, :, None]
    picker = picker.astype(jnp.bfloat16).reshape(devices * slot_count, seq_count)

    def outgoing(weight):
        projected = jnp.dot(normed, weight, preferred_element_type=jnp.float32).astype(jnp.bfloat16)
        placed = jnp.dot(picker, projected, preferred_element_type=jnp.float32).astype(jnp.bfloat16)
        return placed.reshape(devices, slot_count, projected.shape[1])

    send_query = outgoing(w_query)
    send_key = outgoing(w_key)
    send_value = outgoing(w_value)
    send_gate = outgoing(w_gate)
    incoming = (
        lax.all_to_all(send_query, "ep", split_axis=0, concat_axis=0, tiled=True),
        lax.all_to_all(send_key, "ep", split_axis=0, concat_axis=0, tiled=True),
        lax.all_to_all(send_value, "ep", split_axis=0, concat_axis=0, tiled=True),
        lax.all_to_all(send_gate, "ep", split_axis=0, concat_axis=0, tiled=True),
    )
    pair_ids = my_index * pairs_dev + jnp.arange(pairs_dev, dtype=jnp.int32)
    head_pick = (
        jnp.mod(pair_ids, HEADS)[:, None] == jnp.arange(HEADS, dtype=jnp.int32)[None, :]
    ).astype(jnp.bfloat16)
    turns = np.arange(pairs_dev) // HEADS
    pair_rows = np.arange(pairs_dev)

    def arrange(received):
        merged = jnp.dot(head_pick, received.reshape(HEADS, -1), preferred_element_type=jnp.float32)
        merged = merged.reshape(pairs_dev, devices // HEADS, slot_count, received.shape[2])
        return merged[pair_rows, :, turns, :].reshape(pairs_dev, -1).astype(jnp.bfloat16)

    query = arrange(incoming[0])
    key = arrange(incoming[1])
    value = arrange(incoming[2])
    gate = arrange(incoming[3])
    low = jnp.dot(normed, w_low, preferred_element_type=jnp.float32)
    decay_pre = (
        jnp.dot(low, w_decay.astype(jnp.float32), precision=lax.Precision.HIGHEST) + decay_bias
    )
    decay_pre = lax.dynamic_slice_in_dim(
        decay_pre.reshape(seq_count * HEADS, DK), my_index * pairs_dev, pairs_dev, 0
    )
    log_decay = jax.nn.log_sigmoid(decay_pre) / decay_tau
    new_states = (
        head_states * jnp.exp(log_decay)[:, :, None]
        + key.astype(jnp.float32)[:, :, None] * value.astype(jnp.float32)[:, None, :]
    )
    read = jnp.einsum(
        "pk,pkv->pv",
        query.astype(jnp.float32) * DK ** (-0.5),
        new_states,
        precision=lax.Precision.HIGHEST,
    )
    mixed = (rms_scale(read, head_gain) * jax.nn.silu(gate.astype(jnp.float32))).astype(
        jnp.bfloat16
    )
    gathered = lax.all_gather(mixed, "ep", axis=0, tiled=True).reshape(seq_count, HEADS * DV)
    branch = jnp.dot(gathered, w_output, preferred_element_type=jnp.float32).astype(jnp.bfloat16)
    stream = (residual.astype(jnp.float32) + branch.astype(jnp.float32)).astype(jnp.bfloat16)
    floats = stream.astype(jnp.float32)
    total = lax.psum(jnp.sum(floats * floats, axis=1), "ep")
    gain_part = lax.dynamic_slice_in_dim(second_gain, my_index * own_width, own_width)
    scaled = floats * lax.rsqrt(total / width + norm_eps)[:, None] * gain_part.astype(jnp.float32)
    expert_in = lax.all_gather(scaled.astype(jnp.bfloat16), "ep", axis=1, tiled=True)
    capacity = 2 * seq_count * TOP // devices
    weights = route_weights(routes, group_logits, expert_logits, devices // GROUPS)
    hits = (routes == my_index).astype(jnp.int32)
    mine = jnp.sum(weights * hits.astype(jnp.float32), axis=1)
    routed = jnp.sum(hits, axis=1)
    slot = jnp.cumsum(routed) - routed
    chooser = (slot[None, :] == jnp.arange(capacity, dtype=jnp.int32)[:, None]) & (
        routed[None, :] > 0
    )
    picked = jnp.dot(
        chooser.astype(jnp.bfloat16), expert_in, preferred_element_type=jnp.float32
    ).astype(jnp.bfloat16)
    row_weight = jnp.dot(chooser.astype(jnp.float32), mine, precision=lax.Precision.HIGHEST)
    gate_part = jnp.dot(picked, expert_gate[0], preferred_element_type=jnp.float32)
    up_part = jnp.dot(picked, expert_up[0], preferred_element_type=jnp.float32)
    active = (jax.nn.silu(gate_part) * up_part * row_weight[:, None]).astype(jnp.bfloat16)
    expert_rows = jnp.dot(active, expert_down[0], preferred_element_type=jnp.float32).astype(
        jnp.bfloat16
    )
    arrived = lax.all_to_all(expert_rows, "ep", split_axis=1, concat_axis=0, tiled=True)
    every = jnp.arange(devices, dtype=jnp.int32)
    hit_all = jnp.sum((routes[:, :, None] == every[None, None, :]).astype(jnp.int32), axis=1)
    slot_all = jnp.cumsum(hit_all, axis=0) - hit_all
    placer = (slot_all[:, :, None] == jnp.arange(capacity, dtype=jnp.int32)[None, None, :]) & (
        hit_all[:, :, None] > 0
    )
    placer = placer.astype(jnp.bfloat16).reshape(seq_count, devices * capacity)
    returned = jnp.dot(placer, arrived, preferred_element_type=jnp.float32)
    layer_out = (stream.astype(jnp.float32) + returned).astype(jnp.bfloat16)
    return (layer_out, new_states)


def solution(mesh):
    return jax.shard_map(
        per_device,
        mesh=mesh,
        in_specs=(
            P("grp", "ep"),
            P(("grp", "ep"), None, None),
            P(),
            P(None, "ep"),
            P(None, "ep"),
            P(None, "ep"),
            P(None, "ep"),
            P(),
            P(),
            P(),
            P(),
            P(None, "ep"),
            P(),
            P("grp", None),
            P("grp", None),
            P("grp", None),
            P("ep", None, None),
            P("ep", None, None),
            P("ep", None, None),
        ),
        out_specs=(P("grp", "ep"), P(("grp", "ep"), None, None)),
        check_vma=False,
    )
```

profile of v0, /device:TPU:0, one launch (start us, length us, event | category | flops | bytes accessed | tf_op | source)
XLA Modules:
  0.0 169.2 jit_solution(12246803465482614124)
XLA Ops:
  0.7 23.7 %all_gather.9 = bf16[8,4096]{1,0:T(8,128)(2,1)S(1)} all-gather(bf16[8,256]{1,0:T(8,128)(2,1)} %param.29), channel_id=1, replica_groups=mesh['grp'=2,'ep'=16] {'ep'}, dimensions={1}, use_global_device_ids=true | all-gather | bytes 69632 | tf_op jit(solution)/shard_map/all_gather | solution.py:67
  25.3 1.6 fusion.14
  27.5 3.4 %all-to-all-start.1 = ((bf16[16,1,128]{2,1,0:T(2,128)(2,1)}), bf16[16,1,128]{2,1,0:T(2,128)(2,1)S(1)}, u32[]{:S(2)}, u32[]{:S(2)}) async-start(bf16[16,1,128]{2,1,0:T(2,128)(2,1)} %copy.61), calls=%async_computation.1 | async-start | bytes 16384 | tf_op jit(solution)/shard_map/all_to_all | solution.py:89
  33.6 1.1 fusion.88
  34.8 1.0 convolution_add_fusion
  35.8 1.6 fusion.13
  37.4 2.1 %fusion.6 = bf16[16,1,256]{2,0,1:T(8,128)(2,1)S(1)} fusion(bf16[4096,256]{1,0:T(8,128)(2,1)} %param.35, s32[16]{0:T(128)S(1)} %and_select_fusion.1, pred[16]{0:T(512)(128)(4,1)S(1)} %broadcast_compare_fusion.2, bf16[8,4096]{1,0:T(8,128)(2,1)S(1)} %all_gather.9, f32[4096]{0:T(1024)S(1)} %convert_element_type.145, f32[8]{0:T(128)S(1)} %add_rsqrt_fusion.2), kind=kOutput, calls=%fused_computation.16 | convolution fusion | flops 16980224 | bytes 2187376 | tf_op jit(solution)/shard_map/dot_general | solution.py:80
  44.5 6.0 %all-to-all-start = ((bf16[16,1,128]{2,1,0:T(2,128)(2,1)}), bf16[16,1,128]{2,1,0:T(2,128)(2,1)S(1)}, u32[]{:S(2)}, u32[]{:S(2)}) async-start(bf16[16,1,128]{2,1,0:T(2,128)(2,1)} %copy.59), calls=%async_computation | async-start | bytes 16384 | tf_op jit(solution)/shard_map/all_to_all | solution.py:88
  51.3 5.5 %all-to-all-done = bf16[16,1,128]{2,1,0:T(2,128)(2,1)S(1)} async-done(((bf16[16,1,128]{2,1,0:T(2,128)(2,1)}), bf16[16,1,128]{2,1,0:T(2,128)(2,1)S(1)}, u32[]{:S(2)}, u32[]{:S(2)}) %all-to-all-start) | async-done | bytes 4128 | tf_op jit(solution)/shard_map/all_to_all | solution.py:88
  56.8 3.4 %all-to-all-start.2 = ((bf16[16,2,128]{2,1,0:T(2,128)(2,1)}), bf16[16,2,128]{2,1,0:T(2,128)(2,1)S(1)}, u32[]{:S(2)}, u32[]{:S(2)}) async-start(bf16[16,2,128]{2,1,0:T(2,128)(2,1)} %reshape.330), calls=%async_computation.2 | async-start | bytes 16384 | tf_op jit(solution)/shard_map/all_to_all | solution.py:90
  61.1 5.6 %all-to-all-done.2 = bf16[16,2,128]{2,1,0:T(2,128)(2,1)S(1)} async-done(((bf16[16,2,128]{2,1,0:T(2,128)(2,1)}), bf16[16,2,128]{2,1,0:T(2,128)(2,1)S(1)}, u32[]{:S(2)}, u32[]{:S(2)}) %all-to-all-start.2) | async-done | bytes 8224 | tf_op jit(solution)/shard_map/all_to_all | solution.py:90
  66.6 3.5 %all-to-all-start.3 = ((bf16[16,2,128]{2,1,0:T(2,128)(2,1)}), bf16[16,2,128]{2,1,0:T(2,128)(2,1)S(1)}, u32[]{:S(2)}, u32[]{:S(2)}) async-start(bf16[16,2,128]{2,1,0:T(2,128)(2,1)} %reshape.328), calls=%async_computation.3 | async-start | bytes 16384 | tf_op jit(solution)/shard_map/all_to_all | solution.py:91
  71.0 2.7 %multiply_add_fusion = f32[2,512,1024]{2,1,0:T(8,128)S(1)} fusion(f32[2,512,1024]{2,1,0:T(8,128)} %param.30, f32[2,1024]{1,0:T(2,128)S(1)} %bitcast.122, f32[2,512]{1,0:T(2,128)S(1)} %bitcast.124, f32[2,512]{1,0:T(2,128)S(1)} %fusion.44), kind=kLoop, calls=%fused_computation.11 | loop fusion | flops 3145728 | bytes 8404992 | tf_op jit(solution)/shard_map/add | solution.py:118
  73.8 2.0 %copy-done.1 = f32[2,512,1024]{2,1,0:T(8,128)} copy-done((f32[2,512,1024]{2,1,0:T(8,128)}, f32[2,512,1024]{2,1,0:T(8,128)S(1)}, u32[]{:S(2)}) %copy-start.1) | copy-done | bytes 4194328
  75.8 2.1 %fusion.92 = f32[2,1,1024]{2,1,0:T(1,128)S(1)} fusion(f32[2,512,1]{1,2,0:T(1,128)S(1)} %bitcast.123, f32[2,512,1024]{2,1,0:T(8,128)S(1)} %multiply_add_fusion), kind=kOutput, calls=%fused_computation.142 | convolution fusion | flops 12582912 | bytes 4206592 | tf_op jit(solution)/shard_map/pk,pkv->pv/dot_general | solution.py:121
  78.9 21.8 %all-gather = bf16[16,2,1024]{2,1,0:T(2,128)(2,1)S(1)} all-gather(bf16[1,2,1024]{2,1,0:T(2,128)(2,1)S(1)} %fusion.60), channel_id=1, replica_groups=mesh['grp'=2,'ep'=16] {'ep'}, dimensions={0}, use_global_device_ids=true | all-gather | bytes 69632 | tf_op jit(solution)/shard_map/all_gather | solution.py:130
  100.8 2.1 %multiply_reduce_fusion = (f32[8]{0:T(128)S(1)}, f32[8,256]{1,0:T(8,128)S(1)}) fusion(bf16[8,4096]{1,0:T(8,128)(2,1)S(1)} %reshape.284, bf16[4096,256]{1,0:T(8,128)(2,1)} %param.40, bf16[8,256]{1,0:T(8,128)(2,1)S(1)} %copy-done.2), kind=kOutput, calls=%fused_computation.58 | convolution fusion | flops 16793592 | bytes 2175008 | tf_op jit(solution)/shard_map/dot_general | solution.py:131
  102.9 29.8 %psum.7 = f32[8]{0:T(128)S(1)} all-reduce(f32[8]{0:T(128)S(1)} %get-tuple-element.2), channel_id=1, replica_groups=mesh['grp'=2,'ep'=16] {'ep'}, use_global_device_ids=true, to_apply=%region_7.8 | all-reduce | flops 8 | bytes 64 | tf_op jit(solution)/shard_map/psum | solution.py:134
  132.8 17.3 %all_gather.11 = bf16[8,4096]{1,0:T(8,128)(2,1)S(1)} all-gather(bf16[8,256]{1,0:T(8,128)(2,1)S(1)} %multiply_convert_fusion), channel_id=1, replica_groups=mesh['grp'=2,'ep'=16] {'ep'}, dimensions={1}, use_global_device_ids=true | all-gather | bytes 69632 | tf_op jit(solution)/shard_map/all_gather | solution.py:137
  150.2 2.8 %fusion.3 = f32[2,512]{1,0:T(2,128)S(1)} fusion(bf16[2,4096]{1,0:T(2,128)(2,1)S(1)} %convolution_convert_fusion.1, bf16[1,4096,512]{2,1,0:T(8,128)(2,1)} %param.45), kind=kOutput, calls=%fused_computation.9 | convolution fusion | flops 8388608 | bytes 4214784 | tf_op jit(solution)/shard_map/dot_general | solution.py:151
  153.1 5.4 %convolution_convert_fusion = bf16[2,4096]{1,0:T(2,128)(2,1)} fusion(bf16[1,512,4096]{2,1,0:T(8,128)(2,1)} %param.47, bf16[2,4096]{1,0:T(2,128)(2,1)S(1)} %convolution_convert_fusion.1, bf16[1,4096,512]{2,1,0:T(8,128)(2,1)} %param.46, f32[2,512]{1,0:T(2,128)S(1)} %fusion.3, f32[2]{0:T(128)S(1)} %convolution_bitcast_fusion.5), kind=kOutput, calls=%fused_computation.4 | convolution fusion | flops 16792576 | bytes 8425480 | tf_op jit(solution)/shard_map/dot_general | solution.py:154
  158.4 3.5 %all-to-all-start.4 = ((bf16[2,16,256]{2,0,1:T(2,128)(2,1)}), bf16[2,16,256]{2,0,1:T(2,128)(2,1)S(1)}, u32[]{:S(2)}, u32[]{:S(2)}) async-start(bf16[2,16,256]{2,0,1:T(2,128)(2,1)} %bitcast.28), calls=%async_computation.4 | async-start | bytes 32768 | tf_op jit(solution)/shard_map/all_to_all | solution.py:157
  162.0 6.4 %all-to-all-done.4 = bf16[2,16,256]{2,0,1:T(2,128)(2,1)S(1)} async-done(((bf16[2,16,256]{2,0,1:T(2,128)(2,1)}), bf16[2,16,256]{2,0,1:T(2,128)(2,1)S(1)}, u32[]{:S(2)}, u32[]{:S(2)}) %all-to-all-start.4) | async-done | bytes 16416 | tf_op jit(solution)/shard_map/all_to_all | solution.py:157
  168.4 0.8 fusion.8
  (84 shorter events, 13.0 us)
Async XLA Ops:
  0.6 32.5 %copy-start = (bf16[4096,256]{1,0:T(8,128)(2,1)S(1)}, bf16[4096,256]{1,0:T(8,128)(2,1)}, u32[]{:S(2)}) copy-start(bf16[4096,256]{1,0:T(8,128)(2,1)} %param.34) | copy-start | bytes 6291460
  0.6 40.0 %copy-start.3 = (s32[8,2]{0,1:T(2,128)S(1)}, s32[8,2]{0,1:T(2,128)}, u32[]{:S(2)}) copy-start(s32[8,2]{0,1:T(2,128)} %param.42) | copy-start | bytes 196
  0.7 39.1 %copy-start.4 = (f32[8,4]{0,1:T(4,128)S(1)}, f32[8,4]{0,1:T(4,128)}, u32[]{:S(2)}) copy-start(f32[8,4]{0,1:T(4,128)} %param.43) | copy-start | bytes 388
  0.7 39.1 %copy-start.6 = (f32[8,2]{0,1:T(2,128)S(1)}, f32[8,2]{0,1:T(2,128)}, u32[]{:S(2)}) copy-start(f32[8,2]{0,1:T(2,128)} %param.44) | copy-start | bytes 196
  0.7 43.8 %copy-start.5 = (bf16[1024]{0:T(1024)(128)(2,1)S(1)}, bf16[1024]{0:T(1024)(128)(2,1)}, u32[]{:S(2)}) copy-start(bf16[1024]{0:T(1024)(128)(2,1)} %param.39) | copy-start | bytes 6148
  27.5 16.9 %all-to-all-start.1 = ((bf16[16,1,128]{2,1,0:T(2,128)(2,1)}), bf16[16,1,128]{2,1,0:T(2,128)(2,1)S(1)}, u32[]{:S(2)}, u32[]{:S(2)}) async-start(bf16[16,1,128]{2,1,0:T(2,128)(2,1)} %copy.61), calls=%async_computation.1 | async-start | bytes 16384 | tf_op jit(solution)/shard_map/all_to_all | solution.py:89
  44.5 12.3 %all-to-all-start = ((bf16[16,1,128]{2,1,0:T(2,128)(2,1)}), bf16[16,1,128]{2,1,0:T(2,128)(2,1)S(1)}, u32[]{:S(2)}, u32[]{:S(2)}) async-start(bf16[16,1,128]{2,1,0:T(2,128)(2,1)} %copy.59), calls=%async_computation | async-start | bytes 16384 | tf_op jit(solution)/shard_map/all_to_all | solution.py:88
  56.8 9.8 %all-to-all-start.2 = ((bf16[16,2,128]{2,1,0:T(2,128)(2,1)}), bf16[16,2,128]{2,1,0:T(2,128)(2,1)S(1)}, u32[]{:S(2)}, u32[]{:S(2)}) async-start(bf16[16,2,128]{2,1,0:T(2,128)(2,1)} %reshape.330), calls=%async_computation.2 | async-start | bytes 16384 | tf_op jit(solution)/shard_map/all_to_all | solution.py:90
  66.6 11.3 %all-to-all-start.3 = ((bf16[16,2,128]{2,1,0:T(2,128)(2,1)}), bf16[16,2,128]{2,1,0:T(2,128)(2,1)S(1)}, u32[]{:S(2)}, u32[]{:S(2)}) async-start(bf16[16,2,128]{2,1,0:T(2,128)(2,1)} %reshape.328), calls=%async_computation.3 | async-start | bytes 16384 | tf_op jit(solution)/shard_map/all_to_all | solution.py:91
  73.7 2.0 %copy-start.1 = (f32[2,512,1024]{2,1,0:T(8,128)}, f32[2,512,1024]{2,1,0:T(8,128)S(1)}, u32[]{:S(2)}) copy-start(f32[2,512,1024]{2,1,0:T(8,128)S(1)} %multiply_add_fusion) | copy-start | bytes 12582916
  73.8 27.0 %copy-start.2 = (bf16[8,256]{1,0:T(8,128)(2,1)S(1)}, bf16[8,256]{1,0:T(8,128)(2,1)}, u32[]{:S(2)}) copy-start(bf16[8,256]{1,0:T(8,128)(2,1)} %param.29) | copy-start | bytes 12292
  158.4 10.0 %all-to-all-start.4 = ((bf16[2,16,256]{2,0,1:T(2,128)(2,1)}), bf16[2,16,256]{2,0,1:T(2,128)(2,1)S(1)}, u32[]{:S(2)}, u32[]{:S(2)}) async-start(bf16[2,16,256]{2,0,1:T(2,128)(2,1)} %bitcast.28), calls=%async_computation.4 | async-start | bytes 32768 | tf_op jit(solution)/shard_map/all_to_all | solution.py:157
where the time goes:
time: 170 us; the launch traced here: 169 us
  blocking collectives  92.6 us (54%)
  matrix products  22.2 us (13%)
  starting transfers between devices  19.8 us (12%)
  waiting for transfers between devices  17.5 us (10%)
  other arithmetic  8.69 us (5%)
  local copies, waits for them, and re-layouts  7.43 us (4%)
    psum x1, blocking collectives, per_device(): total = lax.psum(jnp.sum(floats * floats, axis=1), 'ep')  29.8 us
    all_gather x1, blocking collectives, per_device(): rows = lax.all_gather(residual, 'ep', axis=1, tiled=True)  23.7 us
    all_gather x1, blocking collectives, per_device(): lax.all_gather(mixed, 'ep', axis=0, tiled=True)  21.8 us
    all_gather x1, blocking collectives, per_device(): lax.all_gather(scaled.astype(jnp.bfloat16), 'ep', axis=1, tiled=True)  17.3 us
    all_to_all x1, waiting for transfers between devices, per_device(): lax.all_to_all(expert_rows, 'ep', split_axis=1, concat_axis=0, tiled=True)  6.42 us
    all_to_all x1, starting transfers between devices, per_device(): lax.all_to_all(send_query, 'ep', split_axis=0, concat_axis=0, tiled=True)  5.98 us
    dot_general x4, matrix products, outgoing(): jnp.dot(picker, projected, preferred_element_type=jnp.float32)  5.92 us
    all_to_all x1, waiting for transfers between devices, per_device(): lax.all_to_all(send_value, 'ep', split_axis=0, concat_axis=0, tiled=True)  5.56 us
  transfers between devices with their start and end apart: 5, of which 3 were waited for; matrix products, arithmetic and copies ran while one was open for 12% of the time, Pallas kernels for 0%

commit v1 on v0

v1 whole, which is shorter than its diff:
```python
import functools

import jax
import jax.numpy as jnp
from jax import lax
from jax.experimental import pallas as pl
from jax.experimental.pallas import tpu as pltpu
from jax.sharding import PartitionSpec as P

HEADS = 4
GROUPS = 4
LANES = 128

norm_eps = 1e-06
decay_tau = 16.0
f32 = jnp.float32
bf16 = jnp.bfloat16

ANY = pl.BlockSpec(memory_space=pl.ANY)
VMEM = pl.BlockSpec(memory_space=pltpu.VMEM)
SMEM = pl.BlockSpec(memory_space=pltpu.SMEM)


def route_weights(routes, group_logits, expert_logits, per_group):
    group_exp = jnp.exp(group_logits)
    group_prob = group_exp / jnp.sum(group_exp, axis=1, keepdims=True)
    chosen = routes[:, 0] // per_group
    groups_row = jnp.arange(group_logits.shape[1], dtype=jnp.int32)
    picked = jnp.sum(
        group_prob * (chosen[:, None] == groups_row[None, :]).astype(f32), axis=1
    )
    expert_exp = jnp.exp(expert_logits)
    return expert_exp / jnp.sum(expert_exp, axis=1, keepdims=True) * picked[:, None]


def start_chunks(pairs, sems, chunks):
    started = []
    for c in range(chunks):
        row = []
        for n, (src, dst) in enumerate(pairs):
            size = src.shape[0] // chunks
            rows = pl.ds(c * size, size)
            copy = pltpu.make_async_copy(src.at[rows], dst.at[rows], sems.at[n, c])
            copy.start()
            row.append(copy)
        started.append(row)
    return started


def normed_rows(blocks_ref, gain_ref):
    count, _, own = blocks_ref.shape
    total = None
    for j in range(count):
        x = blocks_ref[j].astype(f32)
        total = x * x if total is None else total + x * x
    mean = jnp.sum(total, axis=1, keepdims=True) / (count * own)
    scale = lax.rsqrt(mean + norm_eps)
    out = []
    for j in range(count):
        gain = gain_ref[:, j * own : (j + 1) * own].astype(f32)
        out.append((blocks_ref[j].astype(f32) * scale * gain).astype(bf16))
    return jnp.concatenate(out, axis=1)


def project_kernel(
    chunks, blocks_ref, gain_ref, low_w_ref, wq, wk, wv, wg, send_ref, low_ref, bq, bk, bv, bg, sems
):
    started = start_chunks(((wq, bq), (wk, bk), (wv, bv), (wg, bg)), sems, chunks)
    normed = normed_rows(blocks_ref, gain_ref)
    low_ref[...] = lax.dot_general(
        low_w_ref[...], normed, (((1,), (1,)), ((), ())), preferred_element_type=f32
    )
    size = bq.shape[0] // chunks
    sums = [None] * 4
    for c in range(chunks):
        part = normed[:, c * size : (c + 1) * size]
        for n, buf in enumerate((bq, bk, bv, bg)):
            started[c][n].wait()
            one = jnp.dot(part, buf[c * size : (c + 1) * size, :], preferred_element_type=f32)
            sums[n] = one if sums[n] is None else sums[n] + one
    projected = jnp.concatenate(sums, axis=1).astype(bf16).astype(f32)
    rows = projected.shape[1] // LANES
    tokens = projected.shape[0]
    times = send_ref.shape[0] // tokens
    pad = jnp.zeros((send_ref.shape[1] - rows, LANES), f32)
    for s in range(tokens):
        tile = jnp.concatenate(
            [projected[s : s + 1, r * LANES : (r + 1) * LANES] for r in range(rows)] + [pad], axis=0
        )
        for t in range(times):
            send_ref[s * times + t] = tile


def decay_kernel(seq_ref, low_ref, w_ref, bias_ref, out_ref):
    lane = lax.broadcasted_iota(jnp.int32, low_ref.shape, 1)
    low = jnp.sum(jnp.where(lane == seq_ref[0], low_ref[...], 0.0), axis=1, keepdims=True)
    pre = jnp.sum(w_ref[...].astype(f32) * low, axis=0, keepdims=True) + bias_ref[...]
    log_decay = (jnp.minimum(pre, 0.0) - jnp.log1p(jnp.exp(-jnp.abs(pre)))) / decay_tau
    decay = jnp.exp(log_decay)
    wide = out_ref.shape[2]
    for r in range(out_ref.shape[0]):
        out_ref[r] = decay[:, r * wide : (r + 1) * wide]


def tile_columns(tile, decay, qw):
    if qw < LANES:
        decay = jnp.concatenate([decay, jnp.zeros((1, LANES - qw), f32)], axis=1)
    row = lax.broadcasted_iota(jnp.int32, tile.shape, 0)
    turned = jnp.where(row == tile.shape[0] - 1, decay, tile).T
    last = tile.shape[0] - 1

    def column(at):
        return turned[at % LANES : at % LANES + qw, at // LANES : at // LANES + 1]

    return column(0), column(qw), turned[:qw, last : last + 1]


def wide_row(tiles, at, width):
    pieces = []
    for tile in tiles:
        for lane in range(at, at + width, LANES):
            pieces.append(tile[lane // LANES : lane // LANES + 1, :])
    return jnp.concatenate(pieces, axis=1)


def read_kernel(qw, vw, tiles_ref, decay_ref, gain_ref, states, send_ref, buf, sems):
    pairs, dk, dv = states.shape
    sources = dk // qw
    copies = []
    for p in range(pairs):
        for i in range(sources):
            rows = pl.ds(i * qw, qw)
            copy = pltpu.make_async_copy(
                states.at[p, rows], buf.at[p, rows], sems.at[p, i]
            )
            copy.start()
            copies.append(copy)
    lines = []
    for p in range(pairs):
        tiles = [tiles_ref[p * sources + i] for i in range(sources)]
        value = wide_row(tiles, 2 * qw, vw)
        gate = wide_row(tiles, 2 * qw + vw, vw)
        total = jnp.zeros((8, dv), f32)
        both = jnp.zeros((), f32)
        for i in range(sources):
            query, key, decay = tile_columns(tiles[i], decay_ref[p * sources + i], qw)
            both = both + jnp.sum(query * key)
            factor = query * decay
            copies[p * sources + i].wait()
            for g in range(qw // 8):
                at = i * qw + g * 8
                total = total + buf[p, at : at + 8, :] * factor[g * 8 : g * 8 + 8]
        read = (jnp.sum(total, axis=0, keepdims=True) + both * value) * dk ** (-0.5)
        mean = jnp.sum(read * read, axis=1, keepdims=True) / dv
        line = read * lax.rsqrt(mean + norm_eps) * gain_ref[...].astype(f32)
        line = line * (gate * (1.0 / (1.0 + jnp.exp(-gate))))
        lines += [line[:, c * LANES : (c + 1) * LANES] for c in range(dv // LANES)]
    mixed = jnp.concatenate(lines, axis=0).astype(bf16)
    for d in range(send_ref.shape[0]):
        send_ref[d] = mixed


def update_kernel(qw, vw, sources, tiles_ref, decay_ref, state_ref, out_ref):
    p, i = pl.program_id(0), pl.program_id(1)
    tiles = [tiles_ref[p * sources + n] for n in range(sources)]
    value = wide_row(tiles, 2 * qw, vw)
    _, key, decay = tile_columns(tiles_ref[p * sources + i], decay_ref[p * sources + i], qw)
    out_ref[0] = state_ref[0] * decay + key * value


def branch_kernel(chunks, got_ref, res_ref, w, stream_ref, send_ref, buf, sems):
    started = start_chunks(((w, buf),), sems, chunks)
    tokens = res_ref.shape[0]
    parts = got_ref[...].astype(f32).reshape(tokens, -1, LANES)
    parts = jnp.swapaxes(parts, 0, 1)
    size = buf.shape[0] // chunks
    total = None
    for c in range(chunks):
        each = size // LANES
        part = jnp.concatenate([parts[c * each + m] for m in range(each)], axis=1).astype(bf16)
        started[c][0].wait()
        one = jnp.dot(part, buf[c * size : (c + 1) * size, :], preferred_element_type=f32)
        total = one if total is None else total + one
    stream = (res_ref[...].astype(f32) + total.astype(bf16).astype(f32)).astype(bf16)
    stream_ref[...] = stream
    for d in range(send_ref.shape[0]):
        send_ref[d] = stream


def expert_kernel(
    chunks, blocks_ref, gain_ref, share_ref, wg, wu, wd, send_ref, bg, bu, bd, sems, dsems
):
    started = start_chunks(((wg.at[0], bg), (wu.at[0], bu)), sems, chunks)
    own = send_ref.shape[2]
    pieces = 4
    wide = bd.shape[1] // pieces
    downs = []
    for c in range(pieces):
        columns = pl.ds(c * wide, wide)
        copy = pltpu.make_async_copy(wd.at[0, :, columns], bd.at[:, columns], dsems.at[c])
        copy.start()
        downs.append(copy)
    normed = normed_rows(blocks_ref, gain_ref)
    size = bg.shape[0] // chunks
    gate = up = None
    for c in range(chunks):
        part = normed[:, c * size : (c + 1) * size]
        started[c][0].wait()
        one = jnp.dot(part, bg[c * size : (c + 1) * size, :], preferred_element_type=f32)
        gate = one if gate is None else gate + one
        started[c][1].wait()
        one = jnp.dot(part, bu[c * size : (c + 1) * size, :], preferred_element_type=f32)
        up = one if up is None else up + one
    active = gate * (1.0 / (1.0 + jnp.exp(-gate))) * up * share_ref[...]
    active = active.astype(bf16)
    for c in range(pieces):
        downs[c].wait()
        one = jnp.dot(active, bd[:, c * wide : (c + 1) * wide], preferred_element_type=f32)
        one = one.astype(bf16)
        for n in range(wide // own):
            send_ref[c * (wide // own) + n] = one[:, n * own : (n + 1) * own]


def cost(nbytes):
    return pl.CostEstimate(flops=nbytes, bytes_accessed=nbytes, transcendentals=0)


def exchange(blocks):
    return lax.all_to_all(blocks, "ep", split_axis=0, concat_axis=0, tiled=True)


def per_device(
    residual,
    head_states,
    first_gain,
    w_query,
    w_key,
    w_value,
    w_gate,
    w_low,
    w_decay,
    decay_bias,
    head_gain,
    w_output,
    second_gain,
    routes,
    group_logits,
    expert_logits,
    expert_gate,
    expert_up,
    expert_down,
):
    devices = lax.axis_size("ep")
    me = lax.axis_index("ep")
    tokens, own = residual.shape
    width = own * devices
    pairs, dk, dv = head_states.shape
    qw, vw = w_query.shape[1], w_value.shape[1]
    sources = devices // HEADS
    rank = w_low.shape[1]
    ff = expert_gate.shape[2]
    tile = jax.ShapeDtypeStruct

    arrived = exchange(jnp.broadcast_to(residual[None], (devices, tokens, own)))

    first_pair = me * pairs
    first_head = lax.rem(first_pair, HEADS)
    decay_w = lax.dynamic_slice_in_dim(w_decay, first_head * dk, pairs * dk, 1)
    decay_b = lax.dynamic_slice_in_dim(decay_bias, first_head * dk, pairs * dk, 0)
    weights = route_weights(routes, group_logits, expert_logits, devices // GROUPS)
    share = jnp.sum(weights * (routes == me).astype(f32), axis=1)[:, None]

    chunks = 4
    send, low = pl.pallas_call(
        functools.partial(project_kernel, chunks),
        out_shape=(tile((devices, 8, LANES), f32), tile((rank, tokens), f32)),
        in_specs=[VMEM] * 3 + [ANY] * 4,
        out_specs=(VMEM, VMEM),
        scratch_shapes=[
            pltpu.VMEM((width, qw), bf16),
            pltpu.VMEM((width, qw), bf16),
            pltpu.VMEM((width, vw), bf16),
            pltpu.VMEM((width, vw), bf16),
            pltpu.SemaphoreType.DMA((4, chunks)),
        ],
        cost_estimate=cost(width * (qw + vw) * 4),
        name="project",
    )(arrived, first_gain[None, :], w_low.T, w_query, w_key, w_value, w_gate)
    got = exchange(send)

    decay = pl.pallas_call(
        decay_kernel,
        out_shape=tile((pairs * sources, 1, qw), f32),
        in_specs=[SMEM, VMEM, VMEM, VMEM],
        out_specs=VMEM,
        cost_estimate=cost(1 << 20),
        name="decay",
    )((first_pair // HEADS)[None], low, decay_w, decay_b[None, :])

    tiles = lax.dynamic_slice_in_dim(got, first_head * sources, pairs * sources, 0)
    send = pl.pallas_call(
        functools.partial(read_kernel, qw, vw),
        out_shape=tile((devices, pairs * dv // LANES, LANES), bf16),
        in_specs=[VMEM, VMEM, VMEM, ANY],
        out_specs=VMEM,
        scratch_shapes=[
            pltpu.VMEM((pairs, dk, dv), f32),
            pltpu.SemaphoreType.DMA((pairs, sources)),
        ],
        cost_estimate=cost(pairs * dk * dv * 4),
        name="read",
    )(tiles, decay, head_gain[None, :], head_states)
    got = exchange(send)

    block = pl.BlockSpec((1, qw, dv), lambda p, i: (p, i, 0))
    new_states = pl.pallas_call(
        functools.partial(update_kernel, qw, vw, sources),
        grid=(pairs, sources),
        out_shape=tile(head_states.shape, f32),
        in_specs=[VMEM, VMEM, block],
        out_specs=block,
        cost_estimate=cost(pairs * dk * dv * 8),
        name="update",
    )(tiles, decay, head_states)

    stream, send = pl.pallas_call(
        functools.partial(branch_kernel, chunks),
        out_shape=(tile((tokens, own), bf16), tile((devices, tokens, own), bf16)),
        in_specs=[VMEM, VMEM, ANY],
        out_specs=(VMEM, VMEM),
        scratch_shapes=[
            pltpu.VMEM((width, own), bf16),
            pltpu.SemaphoreType.DMA((1, chunks)),
        ],
        cost_estimate=cost(width * own * 2),
        name="branch",
    )(got, residual, w_output)
    got = exchange(send)

    send = pl.pallas_call(
        functools.partial(expert_kernel, 8),
        out_shape=tile((devices, tokens, own), bf16),
        in_specs=[VMEM] * 3 + [ANY] * 3,
        out_specs=VMEM,
        scratch_shapes=[
            pltpu.VMEM((width, ff), bf16),
            pltpu.VMEM((width, ff), bf16),
            pltpu.VMEM((ff, width), bf16),
            pltpu.SemaphoreType.DMA((2, 8)),
            pltpu.SemaphoreType.DMA((4,)),
        ],
        cost_estimate=cost(width * ff * 6),
        name="expert",
    )(got, second_gain[None, :], share, expert_gate, expert_up, expert_down)
    got = exchange(send)
    layer_out = (stream.astype(f32) + jnp.sum(got.astype(f32), axis=0)).astype(bf16)
    return (layer_out, new_states)


def solution(mesh):
    return jax.shard_map(
        per_device,
        mesh=mesh,
        in_specs=(
            P("grp", "ep"),
            P(("grp", "ep"), None, None),
            P(),
            P(None, "ep"),
            P(None, "ep"),
            P(None, "ep"),
            P(None, "ep"),
            P(),
            P(),
            P(),
            P(),
            P(None, "ep"),
            P(),
            P("grp", None),
            P("grp", None),
            P("grp", None),
            P("ep", None, None),
            P("ep", None, None),
            P("ep", None, None),
        ),
        out_specs=(P("grp", "ep"), P(("grp", "ep"), None, None)),
        check_vma=False,
    )
```

time: 170 us -> 83.4 us (0.49)
  blocking collectives: 92.6 us -> 0 us
  Pallas kernels: 0 us -> 29.7 us
  matrix products: 22.2 us -> 0 us
  other arithmetic: 8.69 us -> 0.72 us
  waiting for transfers between devices: 17.5 us -> 21.4 us
    all_gather x3 -> x0, blocking collectives: 62.8 us -> none  [the longest x1 23.7 us: per_device(): rows = lax.all_gather(residual, 'ep', axis=1, tiled=True)]
    psum x1 -> x0, blocking collectives: 29.8 us -> none  [per_device(): total = lax.psum(jnp.sum(floats * floats, axis=1), 'ep')]
    pallas_call x0 -> x6, Pallas kernels: none -> 29.7 us  [the longest x1 7.32 us: per_device(): pl.pallas_call(functools.partial(update_kernel, qw, vw, sources), grid=(p...]
    dot_general x17 -> x0, matrix products: 22.2 us -> none  [the longest x4 5.92 us: outgoing(): jnp.dot(picker, projected, preferred_element_type=jnp.float32)]
    broadcast_in_dim x0 -> x5, local copies, waits for them, and re-layouts: none -> 4.56 us  [the longest x1 1.37 us: per_device(): arrived = exchange(jnp.broadcast_to(residual[None], (devices, tokens, own)))]
    all_to_all x5, waiting for transfers between devices: 17.5 us -> 21.4 us  [exchange(): return lax.all_to_all(blocks, 'ep', split_axis=0, concat_axis=0, tiled=True)]
    add x1 -> x0, other arithmetic: 2.74 us -> none  [per_device(): head_states * jnp.exp(log_decay)[:, :, None]]
    gather x4 -> x0, local copies, waits for them, and re-layouts: 2.29 us -> none  [arrange(): merged[pair_rows, :, turns, :].reshape(pairs_dev, -1).astype(jnp.bfloat16)]
  transfers between devices with their start and end apart: 5 -> 5, of which waited for: 3 -> 4; matrix products, arithmetic and copies ran while one was open for 12% -> 5% of each run, Pallas kernels for 0% -> 11%
where the time goes in v1:
time: 83.4 us; the launch traced here: 82.4 us
  Pallas kernels  29.7 us (36%)
  starting transfers between devices  21.5 us (26%)
  waiting for transfers between devices  21.4 us (26%)
  local copies, waits for them, and re-layouts  8.32 us (10%)
  between operations  0.84 us (1%)
    all_to_all x5, starting transfers between devices, exchange(): return lax.all_to_all(blocks, 'ep', split_axis=0, concat_axis=0, tiled=True)  21.5 us
    all_to_all x5, waiting for transfers between devices, exchange(): return lax.all_to_all(blocks, 'ep', split_axis=0, concat_axis=0, tiled=True)  21.4 us
    pallas_call x1, Pallas kernels, per_device(): pl.pallas_call(functools.partial(update_kernel, qw, vw, sources), grid=(p...  7.32 us
    pallas_call x1, Pallas kernels, per_device(): pl.pallas_call(functools.partial(expert_kernel, 8), out_shape=tile((devic...  7.14 us
    pallas_call x1, Pallas kernels, per_device(): pl.pallas_call(functools.partial(project_kernel, chunks), out_shape=(tile...  5.51 us
    pallas_call x1, Pallas kernels, per_device(): pl.pallas_call(functools.partial(read_kernel, qw, vw), out_shape=tile((de...  4.76 us
    pallas_call x1, Pallas kernels, per_device(): pl.pallas_call(functools.partial(branch_kernel, chunks), out_shape=(tile(...  3.49 us
    unnamed x22, local copies, waits for them, and re-layouts  1.93 us
  transfers between devices with their start and end apart: 5, of which 4 were waited for; matrix products, arithmetic and copies ran while one was open for 5% of the time, Pallas kernels for 11%

profile of v1, /device:TPU:0, one launch (start us, length us, event | category | flops | bytes accessed | tf_op | source)
XLA Modules:
  0.0 82.4 jit_solution(9752535886078993773)
XLA Ops:
  0.7 1.4 %broadcast_in_dim.14 = bf16[16,8,256]{2,1,0:T(8,128)(2,1)} broadcast(bf16[8,256]{1,0:T(8,128)(2,1)} %res_ref.1), dimensions={1,2} | broadcast | bytes 69632 | tf_op jit(solution)/shard_map/broadcast_in_dim | solution.py:264
  2.0 7.4 %all-to-all-start = ((bf16[16,8,256]{2,1,0:T(8,128)(2,1)}), bf16[16,8,256]{2,1,0:T(8,128)(2,1)S(1)}, u32[]{:S(2)}, u32[]{:S(2)}) async-start(bf16[16,8,256]{2,1,0:T(8,128)(2,1)} %broadcast_in_dim.14), calls=%async_computation | async-start | bytes 131072 | tf_op jit(solution)/shard_map/all_to_all | solution.py:229
  9.5 1.3 %broadcast_in_dim.30.gain_ref = bf16[1,4096]{1,0:T(2,128)(2,1)} reshape(bf16[4096]{0:T(1024)(128)(2,1)} %param.21) | data formatting | bytes 16384 | tf_op jit(solution)/shard_map/broadcast_in_dim | solution.py:288
  10.8 5.6 %all-to-all-done.blocks_ref = bf16[16,8,256]{2,1,0:T(8,128)(2,1)S(1)} async-done(((bf16[16,8,256]{2,1,0:T(8,128)(2,1)}), bf16[16,8,256]{2,1,0:T(8,128)(2,1)S(1)}, u32[]{:S(2)}, u32[]{:S(2)}) %all-to-all-start) | async-done | bytes 65568 | tf_op jit(solution)/shard_map/all_to_all | solution.py:229
  16.4 0.6 copy-done.2
  17.0 5.5 %project.1 = (f32[16,8,128]{2,1,0:T(8,128)}, f32[16,8]{1,0:T(8,128)}) custom-call(bf16[16,8,256]{2,1,0:T(8,128)(2,1)} %copy-done.2, bf16[1,4096]{1,0:T(2,128)(2,1)} %broadcast_in_dim.30.gain_ref, bf16[16,4096]{1,0:T(8,128)(2,1)} %bitcast.6, bf16[4096,128]{1,0:T(8,128)(2,1)} %wq.1, bf16[4096,128]{1,0:T(8,128)(2,1)} %wk.1, bf16[4096,256]{1,0:T(8,128)(2,1)} %wv.1, ...), custom_call_target="tpu_custom_call" | custom-call | flops 6291456 | bytes 6291456 | tf_op jit(solution)/shard_map/project/pallas_call | solution.py:274
  22.5 3.5 %all-to-all-start.1 = ((f32[16,8,128]{2,1,0:T(8,128)}), f32[16,8,128]{2,1,0:T(8,128)S(1)}, u32[]{:S(2)}, u32[]{:S(2)}) async-start(f32[16,8,128]{2,1,0:T(8,128)} %get-tuple-element.6), calls=%async_computation.1 | async-start | bytes 131072 | tf_op jit(solution)/shard_map/all_to_all | solution.py:229
  27.3 0.6 constant_dynamic-slice_fusion.w_ref
  27.9 1.5 %decay.1.decay_ref = f32[8,1,128]{2,1,0:T(1,128)} custom-call(s32[1]{0:T(128)} %bitcast.1.seq_ref, f32[16,8]{1,0:T(8,128)} %get-tuple-element.7.low_ref, bf16[16,1024]{1,0:T(8,128)(2,1)} %constant_dynamic-slice_fusion.w_ref, f32[1,1024]{1,0:T(1,128)} %bitcast.7), custom_call_target="tpu_custom_call" | custom-call | flops 1048576 | bytes 1048576 | tf_op jit(solution)/shard_map/decay/pallas_call | solution.py:291
  29.4 3.5 %all-to-all-done.1 = f32[16,8,128]{2,1,0:T(8,128)S(1)} async-done(((f32[16,8,128]{2,1,0:T(8,128)}), f32[16,8,128]{2,1,0:T(8,128)S(1)}, u32[]{:S(2)}, u32[]{:S(2)}) %all-to-all-start.1) | async-done | bytes 65568 | tf_op jit(solution)/shard_map/all_to_all | solution.py:229
  32.9 0.6 constant_dynamic-slice_fusion.1.tiles_ref
  33.5 4.8 %read.1 = bf16[16,16,128]{2,1,0:T(8,128)(2,1)} custom-call(f32[8,8,128]{2,1,0:T(8,128)} %constant_dynamic-slice_fusion.1.tiles_ref, f32[8,1,128]{2,1,0:T(1,128)} %decay.1.decay_ref, bf16[1,1024]{1,0:T(2,128)(2,1)} %broadcast_in_dim.33.gain_ref, f32[2,512,1024]{2,1,0:T(8,128)} %state_ref.1), custom_call_target="tpu_custom_call" | custom-call | flops 4194304 | bytes 4194304 | tf_op jit(solution)/shard_map/read/pallas_call | solution.py:301
  38.3 3.5 %all-to-all-start.2 = ((bf16[16,16,128]{2,1,0:T(8,128)(2,1)}), bf16[16,16,128]{2,1,0:T(8,128)(2,1)S(1)}, u32[]{:S(2)}, u32[]{:S(2)}) async-start(bf16[16,16,128]{2,1,0:T(8,128)(2,1)} %read.1), calls=%async_computation.2 | async-start | bytes 131072 | tf_op jit(solution)/shard_map/all_to_all | solution.py:229
  41.9 6.8 %all-to-all-done.2.got_ref = bf16[16,16,128]{2,1,0:T(8,128)(2,1)S(1)} async-done(((bf16[16,16,128]{2,1,0:T(8,128)(2,1)}), bf16[16,16,128]{2,1,0:T(8,128)(2,1)S(1)}, u32[]{:S(2)}, u32[]{:S(2)}) %all-to-all-start.2) | async-done | bytes 65568 | tf_op jit(solution)/shard_map/all_to_all | solution.py:229
  48.7 0.6 copy-done.3
  49.3 3.5 %branch.1 = (bf16[8,256]{1,0:T(8,128)(2,1)}, bf16[16,8,256]{2,1,0:T(8,128)(2,1)}) custom-call(bf16[16,16,128]{2,1,0:T(8,128)(2,1)} %copy-done.3, bf16[8,256]{1,0:T(8,128)(2,1)} %res_ref.1, bf16[4096,256]{1,0:T(8,128)(2,1)} %w.1), custom_call_target="tpu_custom_call" | custom-call | flops 2097152 | bytes 2097152 | tf_op jit(solution)/shard_map/branch/pallas_call | solution.py:326
  52.8 3.5 %all-to-all-start.3 = ((bf16[16,8,256]{2,1,0:T(8,128)(2,1)}), bf16[16,8,256]{2,1,0:T(8,128)(2,1)S(1)}, u32[]{:S(2)}, u32[]{:S(2)}) async-start(bf16[16,8,256]{2,1,0:T(8,128)(2,1)} %get-tuple-element.9), calls=%async_computation.3 | async-start | bytes 131072 | tf_op jit(solution)/shard_map/all_to_all | solution.py:229
  56.4 0.7 copy.21.share_ref
  57.1 0.6 broadcast_in_dim.34.gain_ref
  57.7 5.5 %all-to-all-done.3.blocks_ref = bf16[16,8,256]{2,1,0:T(8,128)(2,1)S(1)} async-done(((bf16[16,8,256]{2,1,0:T(8,128)(2,1)}), bf16[16,8,256]{2,1,0:T(8,128)(2,1)S(1)}, u32[]{:S(2)}, u32[]{:S(2)}) %all-to-all-start.3) | async-done | bytes 65568 | tf_op jit(solution)/shard_map/all_to_all | solution.py:229
  63.2 0.6 copy-done.1
  63.8 7.1 %expert.1 = bf16[16,8,256]{2,1,0:T(8,128)(2,1)} custom-call(bf16[16,8,256]{2,1,0:T(8,128)(2,1)} %copy-done.1, bf16[1,4096]{1,0:T(2,128)(2,1)} %broadcast_in_dim.34.gain_ref, f32[8,1]{1,0:T(8,128)} %copy.21.share_ref, bf16[1,4096,512]{2,1,0:T(8,128)(2,1)} %wg.3, bf16[1,4096,512]{2,1,0:T(8,128)(2,1)} %wu.1, bf16[1,512,4096]{2,1,0:T(8,128)(2,1)} %wd.1), custom_call_target="tpu_custom_call" | custom-call | flops 12582912 | bytes 12582912 | tf_op jit(solution)/shard_map/expert/pallas_call | solution.py:340
  71.0 3.5 %all-to-all-start.4 = ((bf16[16,8,256]{2,1,0:T(8,128)(2,1)}), bf16[16,8,256]{2,1,0:T(8,128)(2,1)S(1)}, u32[]{:S(2)}, u32[]{:S(2)}) async-start(bf16[16,8,256]{2,1,0:T(8,128)(2,1)} %expert.1), calls=%async_computation.4 | async-start | bytes 131072 | tf_op jit(solution)/shard_map/all_to_all | solution.py:229
  74.5 7.3 %update.1 = f32[2,512,1024]{2,1,0:T(8,128)} custom-call(f32[8,8,128]{2,1,0:T(8,128)} %constant_dynamic-slice_fusion.1.tiles_ref, f32[8,1,128]{2,1,0:T(1,128)} %decay.1.decay_ref, f32[2,512,1024]{2,1,0:T(8,128)} %state_ref.1), custom_call_target="tpu_custom_call" | custom-call | flops 8388608 | bytes 8388608 | tf_op jit(solution)/shard_map/update/pallas_call | solution.py:316
  (29 shorter events, 2.0 us)
Async XLA Ops:
  0.6 26.7 %copy-start = (bf16[16,2048]{1,0:T(8,128)(2,1)S(1)}, bf16[16,2048]{1,0:T(8,128)(2,1)}, u32[]{:S(2)}) copy-start(bf16[16,2048]{1,0:T(8,128)(2,1)} %param.27) | copy-start | bytes 196612
  0.6 25.4 %copy-start.9 = (s32[8,2]{0,1:T(2,128)S(1)}, s32[8,2]{0,1:T(2,128)}, u32[]{:S(2)}) copy-start(s32[8,2]{0,1:T(2,128)} %param.32) | copy-start | bytes 196
  0.7 25.4 %copy-start.7 = (bf16[1024]{0:T(1024)(128)(2,1)S(1)}, bf16[1024]{0:T(1024)(128)(2,1)}, u32[]{:S(2)}) copy-start(bf16[1024]{0:T(1024)(128)(2,1)} %param.29) | copy-start | bytes 6148
  0.7 26.0 %copy-start.8 = (f32[2048]{0:T(1024)S(1)}, f32[2048]{0:T(1024)}, u32[]{:S(2)}) copy-start(f32[2048]{0:T(1024)} %param.28) | copy-start | bytes 24580
  2.0 14.3 %all-to-all-start = ((bf16[16,8,256]{2,1,0:T(8,128)(2,1)}), bf16[16,8,256]{2,1,0:T(8,128)(2,1)S(1)}, u32[]{:S(2)}, u32[]{:S(2)}) async-start(bf16[16,8,256]{2,1,0:T(8,128)(2,1)} %broadcast_in_dim.14), calls=%async_computation | async-start | bytes 131072 | tf_op jit(solution)/shard_map/all_to_all | solution.py:229
  16.4 0.6 copy-start.2
  17.0 24.8 %copy-start.5 = (f32[8,4]{0,1:T(4,128)S(1)}, f32[8,4]{0,1:T(4,128)}, u32[]{:S(2)}) copy-start(f32[8,4]{0,1:T(4,128)} %param.33) | copy-start | bytes 388
  22.5 33.8 %copy-start.10 = (f32[8,2]{0,1:T(2,128)S(1)}, f32[8,2]{0,1:T(2,128)}, u32[]{:S(2)}) copy-start(f32[8,2]{0,1:T(2,128)} %param.34) | copy-start | bytes 196
  22.5 34.5 %copy-start.4 = (bf16[4096]{0:T(1024)(128)(2,1)S(1)}, bf16[4096]{0:T(1024)(128)(2,1)}, u32[]{:S(2)}) copy-start(bf16[4096]{0:T(1024)(128)(2,1)} %param.31) | copy-start | bytes 24580
  22.5 10.4 %all-to-all-start.1 = ((f32[16,8,128]{2,1,0:T(8,128)}), f32[16,8,128]{2,1,0:T(8,128)S(1)}, u32[]{:S(2)}, u32[]{:S(2)}) async-start(f32[16,8,128]{2,1,0:T(8,128)} %get-tuple-element.6), calls=%async_computation.1 | async-start | bytes 131072 | tf_op jit(solution)/shard_map/all_to_all | solution.py:229
  38.3 10.4 %all-to-all-start.2 = ((bf16[16,16,128]{2,1,0:T(8,128)(2,1)}), bf16[16,16,128]{2,1,0:T(8,128)(2,1)S(1)}, u32[]{:S(2)}, u32[]{:S(2)}) async-start(bf16[16,16,128]{2,1,0:T(8,128)(2,1)} %read.1), calls=%async_computation.2 | async-start | bytes 131072 | tf_op jit(solution)/shard_map/all_to_all | solution.py:229
  48.7 0.6 copy-start.3
  52.8 10.4 %all-to-all-start.3 = ((bf16[16,8,256]{2,1,0:T(8,128)(2,1)}), bf16[16,8,256]{2,1,0:T(8,128)(2,1)S(1)}, u32[]{:S(2)}, u32[]{:S(2)}) async-start(bf16[16,8,256]{2,1,0:T(8,128)(2,1)} %get-tuple-element.9), calls=%async_computation.3 | async-start | bytes 131072 | tf_op jit(solution)/shard_map/all_to_all | solution.py:229
  63.2 0.6 copy-start.1
  71.0 10.8 %all-to-all-start.4 = ((bf16[16,8,256]{2,1,0:T(8,128)(2,1)}), bf16[16,8,256]{2,1,0:T(8,128)(2,1)S(1)}, u32[]{:S(2)}, u32[]{:S(2)}) async-start(bf16[16,8,256]{2,1,0:T(8,128)(2,1)} %expert.1), calls=%async_computation.4 | async-start | bytes 131072 | tf_op jit(solution)/shard_map/all_to_all | solution.py:229
  74.5 7.4 %copy-start.6 = (bf16[8,256]{1,0:T(8,128)(2,1)S(1)}, bf16[8,256]{1,0:T(8,128)(2,1)}, u32[]{:S(2)}) copy-start(bf16[8,256]{1,0:T(8,128)(2,1)} %get-tuple-element.8) | copy-start | bytes 12292

commit v2 on v1

--- a/solution.py
+++ b/solution.py
@@ -10,6 +10,8 @@
 HEADS = 4
 GROUPS = 4
 LANES = 128
+PC, BC, EC, DC = 2, 1, 2, 1
+UC, UD = 4, 2
 
 norm_eps = 1e-06
 decay_tau = 16.0
@@ -33,7 +35,7 @@
     return expert_exp / jnp.sum(expert_exp, axis=1, keepdims=True) * picked[:, None]
 
 
-def start_chunks(pairs, sems, chunks):
+def start_chunks(pairs, sems, chunks, both=True):
     started = []
     for c in range(chunks):
         row = []
@@ -41,10 +43,26 @@
             size = src.shape[0] // chunks
             rows = pl.ds(c * size, size)
             copy = pltpu.make_async_copy(src.at[rows], dst.at[rows], sems.at[n, c])
-            copy.start()
+            copy.start(priority=(n + c) % 2 if both else 0)
             row.append(copy)
         started.append(row)
     return started
+
+
+def side_by_side(arrays, buf):
+    out, at = [], 0
+    for array in arrays:
+        wide = array.shape[1]
+        out.append((array, buf.at[:, at : at + wide]))
+        at += wide
+    return out
+
+
+def start_small(pairs, sems):
+    copies = [pltpu.make_async_copy(src, dst, sems.at[n]) for n, (src, dst) in enumerate(pairs)]
+    for copy in copies:
+        copy.start()
+    return copies
 
 
 def normed_rows(blocks_ref, gain_ref):
@@ -63,22 +81,44 @@
 
 
 def project_kernel(
-    chunks, blocks_ref, gain_ref, low_w_ref, wq, wk, wv, wg, send_ref, low_ref, bq, bk, bv, bg, sems
+    chunks,
+    blocks,
+    gain,
+    low_w,
+    wq,
+    wk,
+    wv,
+    wg,
+    send_ref,
+    low_ref,
+    *scratch,
 ):
-    started = start_chunks(((wq, bq), (wk, bk), (wv, bv), (wg, bg)), sems, chunks)
+    *bufs, sems, blocks_ref, gain_ref, low_w_ref, small_sems = scratch
+    small = start_small(
+        ((blocks, blocks_ref), (gain, gain_ref), (low_w, low_w_ref)), small_sems
+    )
+    held = [(wq, wk, wv, wg)] if len(bufs) == 1 else [(wq,), (wk,), (wv, wg)]
+    places = []
+    for arrays, buf in zip(held, bufs):
+        places += side_by_side(arrays, buf) if len(arrays) > 1 else [(arrays[0], buf)]
+    started = start_chunks(places, sems, chunks)
+    for copy in small:
+        copy.wait()
     normed = normed_rows(blocks_ref, gain_ref)
     low_ref[...] = lax.dot_general(
         low_w_ref[...], normed, (((1,), (1,)), ((), ())), preferred_element_type=f32
     )
-    size = bq.shape[0] // chunks
-    sums = [None] * 4
+    size = bufs[0].shape[0] // chunks
+    sums = [None] * len(bufs)
     for c in range(chunks):
+        for copy in started[c]:
+            copy.wait()
         part = normed[:, c * size : (c + 1) * size]
-        for n, buf in enumerate((bq, bk, bv, bg)):
-            started[c][n].wait()
+        for n, buf in enumerate(bufs):
             one = jnp.dot(part, buf[c * size : (c + 1) * size, :], preferred_element_type=f32)
             sums[n] = one if sums[n] is None else sums[n] + one
-    projected = jnp.concatenate(sums, axis=1).astype(bf16).astype(f32)
+    total = jnp.concatenate(sums, axis=1)
+    projected = total.astype(bf16).astype(f32)
     rows = projected.shape[1] // LANES
     tokens = projected.shape[0]
     times = send_ref.shape[0] // tokens
@@ -91,7 +131,7 @@
             send_ref[s * times + t] = tile
 
 
-def decay_kernel(seq_ref, low_ref, w_ref, bias_ref, out_ref):
+def decay_kernel(seq_ref, low_ref, w_ref, bias_ref, _gain, _share, out_ref):
     lane = lax.broadcasted_iota(jnp.int32, low_ref.shape, 1)
     low = jnp.sum(jnp.where(lane == seq_ref[0], low_ref[...], 0.0), axis=1, keepdims=True)
     pre = jnp.sum(w_ref[...].astype(f32) * low, axis=0, keepdims=True) + bias_ref[...]
@@ -123,9 +163,13 @@
     return jnp.concatenate(pieces, axis=1)
 
 
-def read_kernel(qw, vw, tiles_ref, decay_ref, gain_ref, states, send_ref, buf, sems):
+def read_kernel(
+    qw, vw, base, got, decay, gain, states, send_ref, buf, sems, tiles_ref, decay_ref, gain_ref, small_sems
+):
     pairs, dk, dv = states.shape
     sources = dk // qw
+    mine = got.at[pl.ds(base[0], pairs * sources)]
+    small = start_small(((mine, tiles_ref), (decay, decay_ref), (gain, gain_ref)), small_sems)
     copies = []
     for p in range(pairs):
         for i in range(sources):
@@ -133,18 +177,20 @@
             copy = pltpu.make_async_copy(
                 states.at[p, rows], buf.at[p, rows], sems.at[p, i]
             )
-            copy.start()
+            copy.start(priority=i % 2)
             copies.append(copy)
+    for copy in small:
+        copy.wait()
     lines = []
     for p in range(pairs):
         tiles = [tiles_ref[p * sources + i] for i in range(sources)]
         value = wide_row(tiles, 2 * qw, vw)
         gate = wide_row(tiles, 2 * qw + vw, vw)
         total = jnp.zeros((8, dv), f32)
-        both = jnp.zeros((), f32)
+        both = jnp.zeros((1, 1), f32)
         for i in range(sources):
             query, key, decay = tile_columns(tiles[i], decay_ref[p * sources + i], qw)
-            both = both + jnp.sum(query * key)
+            both = both + jnp.sum(query * key, axis=0, keepdims=True)
             factor = query * decay
             copies[p * sources + i].wait()
             for g in range(qw // 8):
@@ -160,16 +206,24 @@
         send_ref[d] = mixed
 
 
-def update_kernel(qw, vw, sources, tiles_ref, decay_ref, state_ref, out_ref):
-    p, i = pl.program_id(0), pl.program_id(1)
-    tiles = [tiles_ref[p * sources + n] for n in range(sources)]
+def update_kernel(qw, vw, sources, first, base, tiles_ref, decay_ref, state_ref, *rest):
+    out_ref, flag_ref = rest[-2:]
+    at = first + pl.program_id(0)
+    pair = at // sources * sources
+    tiles = [tiles_ref[base[0] + pair + n] for n in range(sources)]
     value = wide_row(tiles, 2 * qw, vw)
-    _, key, decay = tile_columns(tiles_ref[p * sources + i], decay_ref[p * sources + i], qw)
+    _, key, decay = tile_columns(tiles_ref[base[0] + at], decay_ref[at], qw)
+    flag_ref[...] = jnp.zeros_like(flag_ref)
     out_ref[0] = state_ref[0] * decay + key * value
 
 
-def branch_kernel(chunks, got_ref, res_ref, w, stream_ref, send_ref, buf, sems):
+def branch_kernel(
+    chunks, got, res, w, flag, stream_ref, send_ref, buf, sems, got_ref, res_ref, small_sems
+):
+    small = start_small(((got, got_ref), (res, res_ref)), small_sems)
     started = start_chunks(((w, buf),), sems, chunks)
+    for copy in small:
+        copy.wait()
     tokens = res_ref.shape[0]
     parts = got_ref[...].astype(f32).reshape(tokens, -1, LANES)
     parts = jnp.swapaxes(parts, 0, 1)
@@ -188,11 +242,30 @@
 
 
 def expert_kernel(
-    chunks, blocks_ref, gain_ref, share_ref, wg, wu, wd, send_ref, bg, bu, bd, sems, dsems
+    chunks,
+    blocks,
+    gain,
+    share,
+    wg,
+    wu,
+    wd,
+    flag,
+    send_ref,
+    buf,
+    bd,
+    sems,
+    dsems,
+    blocks_ref,
+    gain_ref,
+    share_ref,
+    small_sems,
 ):
-    started = start_chunks(((wg.at[0], bg), (wu.at[0], bu)), sems, chunks)
+    small = start_small(
+        ((blocks, blocks_ref), (gain, gain_ref), (share, share_ref)), small_sems
+    )
+    started = start_chunks(side_by_side((wg.at[0], wu.at[0]), buf), sems, chunks, False)
     own = send_ref.shape[2]
-    pieces = 4
+    pieces = DC
     wide = bd.shape[1] // pieces
     downs = []
     for c in range(pieces):
@@ -200,17 +273,19 @@
         copy = pltpu.make_async_copy(wd.at[0, :, columns], bd.at[:, columns], dsems.at[c])
         copy.start()
         downs.append(copy)
+    for copy in small:
+        copy.wait()
     normed = normed_rows(blocks_ref, gain_ref)
-    size = bg.shape[0] // chunks
-    gate = up = None
+    size = buf.shape[0] // chunks
+    total = None
     for c in range(chunks):
+        for copy in started[c]:
+            copy.wait()
         part = normed[:, c * size : (c + 1) * size]
-        started[c][0].wait()
-        one = jnp.dot(part, bg[c * size : (c + 1) * size, :], preferred_element_type=f32)
-        gate = one if gate is None else gate + one
-        started[c][1].wait()
-        one = jnp.dot(part, bu[c * size : (c + 1) * size, :], preferred_element_type=f32)
-        up = one if up is None else up + one
+        one = jnp.dot(part, buf[c * size : (c + 1) * size, :], preferred_element_type=f32)
+        total = one if total is None else total + one
+    ff = buf.shape[1] // 2
+    gate, up = total[:, :ff], total[:, ff:]
     active = gate * (1.0 / (1.0 + jnp.exp(-gate))) * up * share_ref[...]
     active = active.astype(bf16)
     for c in range(pieces):
@@ -219,6 +294,10 @@
         one = one.astype(bf16)
         for n in range(wide // own):
             send_ref[c * (wide // own) + n] = one[:, n * own : (n + 1) * own]
+
+
+def grant(mib):
+    return pltpu.CompilerParams(vmem_limit_bytes=mib << 20)
 
 
 def cost(nbytes):
@@ -270,19 +349,23 @@
     weights = route_weights(routes, group_logits, expert_logits, devices // GROUPS)
     share = jnp.sum(weights * (routes == me).astype(f32), axis=1)[:, None]
 
-    chunks = 4
+    gain_row = second_gain[None, :]
+    chunks = PC
+    columns = [2 * (qw + vw)] if qw % LANES == 0 else [qw, qw, 2 * vw]
     send, low = pl.pallas_call(
         functools.partial(project_kernel, chunks),
         out_shape=(tile((devices, 8, LANES), f32), tile((rank, tokens), f32)),
-        in_specs=[VMEM] * 3 + [ANY] * 4,
+        in_specs=[ANY] * 7,
         out_specs=(VMEM, VMEM),
         scratch_shapes=[
-            pltpu.VMEM((width, qw), bf16),
-            pltpu.VMEM((width, qw), bf16),
-            pltpu.VMEM((width, vw), bf16),
-            pltpu.VMEM((width, vw), bf16),
+            *[pltpu.VMEM((width, n), bf16) for n in columns],
             pltpu.SemaphoreType.DMA((4, chunks)),
+            pltpu.VMEM((devices, tokens, own), bf16),
+            pltpu.VMEM((1, width), bf16),
+            pltpu.VMEM((rank, width), bf16),
+            pltpu.SemaphoreType.DMA((3,)),
         ],
+        compiler_params=grant(60),
         cost_estimate=cost(width * (qw + vw) * 4),
         name="project",
     )(arrived, first_gain[None, :], w_low.T, w_query, w_key, w_value, w_gate)
@@ -291,68 +374,96 @@
     decay = pl.pallas_call(
         decay_kernel,
         out_shape=tile((pairs * sources, 1, qw), f32),
-        in_specs=[SMEM, VMEM, VMEM, VMEM],
+        in_specs=[SMEM, VMEM, VMEM, VMEM, ANY, ANY],
         out_specs=VMEM,
+        compiler_params=grant(60),
         cost_estimate=cost(1 << 20),
         name="decay",
-    )((first_pair // HEADS)[None], low, decay_w, decay_b[None, :])
-
-    tiles = lax.dynamic_slice_in_dim(got, first_head * sources, pairs * sources, 0)
+    )((first_pair // HEADS)[None], low, decay_w, decay_b[None, :], gain_row, share)
+
+    base = (first_head * sources)[None]
+    qkvg = got
     send = pl.pallas_call(
         functools.partial(read_kernel, qw, vw),
         out_shape=tile((devices, pairs * dv // LANES, LANES), bf16),
-        in_specs=[VMEM, VMEM, VMEM, ANY],
+        in_specs=[SMEM, ANY, ANY, ANY, ANY],
         out_specs=VMEM,
         scratch_shapes=[
             pltpu.VMEM((pairs, dk, dv), f32),
             pltpu.SemaphoreType.DMA((pairs, sources)),
+            pltpu.VMEM((pairs * sources, 8, LANES), f32),
+            pltpu.VMEM((pairs * sources, 1, qw), f32),
+            pltpu.VMEM((1, dv), bf16),
+            pltpu.SemaphoreType.DMA((3,)),
         ],
+        compiler_params=grant(60),
         cost_estimate=cost(pairs * dk * dv * 4),
         name="read",
-    )(tiles, decay, head_gain[None, :], head_states)
+    )(base, qkvg, decay, head_gain[None, :], head_states)
     got = exchange(send)
 
-    block = pl.BlockSpec((1, qw, dv), lambda p, i: (p, i, 0))
-    new_states = pl.pallas_call(
-        functools.partial(update_kernel, qw, vw, sources),
-        grid=(pairs, sources),
-        out_shape=tile(head_states.shape, f32),
-        in_specs=[VMEM, VMEM, block],
-        out_specs=block,
-        cost_estimate=cost(pairs * dk * dv * 8),
-        name="update",
-    )(tiles, decay, head_states)
+    def update(states, after, first, count):
+        block = pl.BlockSpec(
+            (1, qw, dv), lambda n: ((first + n) // sources, (first + n) % sources, 0)
+        )
+        held = [] if states is None else [states]
+        return pl.pallas_call(
+            functools.partial(update_kernel, qw, vw, sources, first),
+            grid=(count,),
+            out_shape=(tile(head_states.shape, f32), tile((8, LANES), f32)),
+            in_specs=[SMEM, VMEM, VMEM, block, ANY] + [ANY] * len(held),
+            out_specs=(block, pl.BlockSpec((8, LANES), lambda n: (0, 0))),
+            input_output_aliases={5: 0} if held else {},
+            compiler_params=grant(60),
+            cost_estimate=cost(count * qw * dv * 8),
+            name="update",
+        )(base, qkvg, decay, head_states, after, *held)
+
+    blocks = pairs * sources
+    new_states, flag = update(None, send, 0, UC * blocks // 8)
 
     stream, send = pl.pallas_call(
-        functools.partial(branch_kernel, chunks),
+        functools.partial(branch_kernel, BC),
         out_shape=(tile((tokens, own), bf16), tile((devices, tokens, own), bf16)),
-        in_specs=[VMEM, VMEM, ANY],
+        in_specs=[ANY] * 4,
         out_specs=(VMEM, VMEM),
         scratch_shapes=[
             pltpu.VMEM((width, own), bf16),
-            pltpu.SemaphoreType.DMA((1, chunks)),
+            pltpu.SemaphoreType.DMA((1, BC)),
+            pltpu.VMEM(got.shape, bf16),
+            pltpu.VMEM((tokens, own), bf16),
+            pltpu.SemaphoreType.DMA((2,)),
         ],
+        compiler_params=grant(60),
         cost_estimate=cost(width * own * 2),
         name="branch",
-    )(got, residual, w_output)
+    )(got, residual, w_output, flag)
     got = exchange(send)
+    new_states, flag = update(new_states, send, UC * blocks // 8, UD * blocks // 8)
 
     send = pl.pallas_call(
-        functools.partial(expert_kernel, 8),
+        functools.partial(expert_kernel, EC),
         out_shape=tile((devices, tokens, own), bf16),
-        in_specs=[VMEM] * 3 + [ANY] * 3,
+        in_specs=[ANY] * 7,
         out_specs=VMEM,
         scratch_shapes=[
-            pltpu.VMEM((width, ff), bf16),
-            pltpu.VMEM((width, ff), bf16),
+            pltpu.VMEM((width, 2 * ff), bf16),
             pltpu.VMEM((ff, width), bf16),
-            pltpu.SemaphoreType.DMA((2, 8)),
-            pltpu.SemaphoreType.DMA((4,)),
+            pltpu.SemaphoreType.DMA((2, EC)),
+            pltpu.SemaphoreType.DMA((DC,)),
+            pltpu.VMEM((devices, tokens, own), bf16),
+            pltpu.VMEM((1, width), bf16),
+            pltpu.VMEM((tokens, 1), f32),
+            pltpu.SemaphoreType.DMA((3,)),
         ],
+        compiler_params=grant(60),
         cost_estimate=cost(width * ff * 6),
         name="expert",
-    )(got, second_gain[None, :], share, expert_gate, expert_up, expert_down)
+    )(got, gain_row, share, expert_gate, expert_up, expert_down, flag)
     got = exchange(send)
+    if UC + UD < 8:
+        done = (UC + UD) * blocks // 8
+        new_states, _ = update(new_states, send, done, blocks - done)
     layer_out = (stream.astype(f32) + jnp.sum(got.astype(f32), axis=0)).astype(bf16)
     return (layer_out, new_states)
 

time: 83.4 us -> 79.4 us (0.952)
  waiting for transfers between devices: 21.4 us -> 16.8 us
  other arithmetic: 0.72 us -> 3.44 us
  Pallas kernels: 29.7 us -> 27.6 us
    all_to_all x5, waiting for transfers between devices: 21.4 us -> 16.8 us  [exchange(): return lax.all_to_all(blocks, 'ep', split_axis=0, concat_axis=0, tiled=True)]
    pallas_call x1, Pallas kernels: 5.51 us -> 4.56 us  [per_device(): pl.pallas_call(functools.partial(project_kernel, chunks), out_shape=(tile...]
    pallas_call x3 -> x5, Pallas kernels: 17.9 us -> 17.6 us  [the longest x3 8.87 us: update(): pl.pallas_call(functools.partial(update_kernel, qw, vw, sources, first),...]
  transfers between devices with their start and end apart: 5 -> 5, of which waited for: 4 -> 5; matrix products, arithmetic and copies ran while one was open for 5% -> 9% of each run, Pallas kernels for 11% -> 13%
where the time goes in v2:
time: 79.4 us; the launch traced here: 78.6 us
  Pallas kernels  27.6 us (35%)
  starting transfers between devices  21.7 us (27%)
  waiting for transfers between devices  16.8 us (21%)
  local copies, waits for them, and re-layouts  8.3 us (10%)
  other arithmetic  3.44 us (4%)
  between operations  0.81 us (1%)
    all_to_all x5, starting transfers between devices, exchange(): return lax.all_to_all(blocks, 'ep', split_axis=0, concat_axis=0, tiled=True)  21.7 us
    all_to_all x5, waiting for transfers between devices, exchange(): return lax.all_to_all(blocks, 'ep', split_axis=0, concat_axis=0, tiled=True)  16.8 us
    pallas_call x3, Pallas kernels, update(): pl.pallas_call(functools.partial(update_kernel, qw, vw, sources, first),...  8.87 us
    pallas_call x1, Pallas kernels, per_device(): pl.pallas_call(functools.partial(expert_kernel, EC), out_shape=tile((devi...  6.05 us
    pallas_call x1, Pallas kernels, per_device(): pl.pallas_call(functools.partial(project_kernel, chunks), out_shape=(tile...  4.56 us
    pallas_call x1, Pallas kernels, per_device(): pl.pallas_call(functools.partial(read_kernel, qw, vw), out_shape=tile((de...  3.95 us
    pallas_call x1, Pallas kernels, per_device(): pl.pallas_call(functools.partial(branch_kernel, BC), out_shape=(tile((tok...  2.69 us
    unnamed x22, local copies, waits for them, and re-layouts  2.53 us
  transfers between devices with their start and end apart: 5, of which 5 were waited for; matrix products, arithmetic and copies ran while one was open for 9% of the time, Pallas kernels for 13%

profile of v2, /device:TPU:0, one launch (start us, length us, event | category | flops | bytes accessed | tf_op | source)
XLA Modules:
  0.0 78.6 jit_solution(8389423418746263765)
XLA Ops:
  0.7 1.4 %broadcast_in_dim.33 = bf16[16,8,256]{2,1,0:T(8,128)(2,1)} broadcast(bf16[8,256]{1,0:T(8,128)(2,1)} %res.1), dimensions={1,2} | broadcast | bytes 69632 | tf_op jit(solution)/shard_map/broadcast_in_dim | solution.py:343
  2.1 7.4 %all-to-all-start = ((bf16[16,8,256]{2,1,0:T(8,128)(2,1)}), bf16[16,8,256]{2,1,0:T(8,128)(2,1)S(1)}, u32[]{:S(2)}, u32[]{:S(2)}) async-start(bf16[16,8,256]{2,1,0:T(8,128)(2,1)} %broadcast_in_dim.33), calls=%async_computation | async-start | bytes 131072 | tf_op jit(solution)/shard_map/all_to_all | solution.py:308
  9.5 0.7 fusion.2
  10.2 0.7 exponential_reduce_fusion
  10.9 0.7 exponential_reduce_fusion.1
  11.6 1.3 %broadcast_in_dim.34.gain = bf16[1,4096]{1,0:T(2,128)(2,1)} reshape(bf16[4096]{0:T(1024)(128)(2,1)} %param.21) | data formatting | bytes 16384 | tf_op jit(solution)/shard_map/broadcast_in_dim | solution.py:371
  12.9 0.7 fusion
  13.6 2.8 %all-to-all-done.blocks = bf16[16,8,256]{2,1,0:T(8,128)(2,1)S(1)} async-done(((bf16[16,8,256]{2,1,0:T(8,128)(2,1)}), bf16[16,8,256]{2,1,0:T(8,128)(2,1)S(1)}, u32[]{:S(2)}, u32[]{:S(2)}) %all-to-all-start) | async-done | bytes 65568 | tf_op jit(solution)/shard_map/all_to_all | solution.py:308
  17.0 4.6 %project.1 = (f32[16,8,128]{2,1,0:T(8,128)}, f32[16,8]{1,0:T(8,128)}) custom-call(bf16[16,8,256]{2,1,0:T(8,128)(2,1)} %copy-done.2, bf16[1,4096]{1,0:T(2,128)(2,1)} %broadcast_in_dim.34.gain, bf16[16,4096]{1,0:T(8,128)(2,1)} %bitcast.7, bf16[4096,128]{1,0:T(8,128)(2,1)} %wq.1, bf16[4096,128]{1,0:T(8,128)(2,1)} %wk.1, bf16[4096,256]{1,0:T(8,128)(2,1)} %wv.1, ...), custom_call_target="tpu_custom_call" | custom-call | flops 6291456 | bytes 6291456 | tf_op jit(solution)/shard_map/project/pallas_call | solution.py:355
  21.6 3.5 %all-to-all-start.1 = ((f32[16,8,128]{2,1,0:T(8,128)}), f32[16,8,128]{2,1,0:T(8,128)S(1)}, u32[]{:S(2)}, u32[]{:S(2)}) async-start(f32[16,8,128]{2,1,0:T(8,128)} %get-tuple-element.11), calls=%async_computation.1 | async-start | bytes 131072 | tf_op jit(solution)/shard_map/all_to_all | solution.py:308
  28.3 1.5 %decay.1.decay_ref = f32[8,1,128]{2,1,0:T(1,128)} custom-call(s32[1]{0:T(128)} %bitcast.2.seq_ref, f32[16,8]{1,0:T(8,128)} %get-tuple-element.12.low_ref, bf16[16,1024]{1,0:T(8,128)(2,1)} %constant_dynamic-slice_fusion.w_ref, f32[1,1024]{1,0:T(1,128)} %bitcast.8, bf16[1,4096]{1,0:T(2,128)(2,1)} %broadcast_in_dim.37._gain.gain, f32[8,1]{1,0:T(8,128)} %copy.23._share.share), custom_call_target="tpu_custom_call" | custom-call | flops 1048576 | bytes 1048576 | tf_op jit(solution)/shard_map/decay/pallas_call | solution.py:374
  29.7 2.2 %all-to-all-done.1.got.tiles_ref = f32[16,8,128]{2,1,0:T(8,128)S(1)} async-done(((f32[16,8,128]{2,1,0:T(8,128)}), f32[16,8,128]{2,1,0:T(8,128)S(1)}, u32[]{:S(2)}, u32[]{:S(2)}) %all-to-all-start.1) | async-done | bytes 65568 | tf_op jit(solution)/shard_map/all_to_all | solution.py:308
  32.6 3.9 %read.1.rest_0_ = bf16[16,16,128]{2,1,0:T(8,128)(2,1)} custom-call(s32[1]{0:T(128)} %bitcast.base, f32[16,8,128]{2,1,0:T(8,128)} %copy-done.1, f32[8,1,128]{2,1,0:T(1,128)} %decay.1.decay_ref, bf16[1,1024]{1,0:T(2,128)(2,1)} %broadcast_in_dim.39.gain, f32[2,512,1024]{2,1,0:T(8,128)} %state_ref.5), custom_call_target="tpu_custom_call" | custom-call | flops 4194304 | bytes 4194304 | tf_op jit(solution)/shard_map/read/pallas_call | solution.py:386
  36.5 3.8 %all-to-all-start.2 = ((bf16[16,16,128]{2,1,0:T(8,128)(2,1)}), bf16[16,16,128]{2,1,0:T(8,128)(2,1)S(1)}, u32[]{:S(2)}, u32[]{:S(2)}) async-start(bf16[16,16,128]{2,1,0:T(8,128)(2,1)} %read.1.rest_0_), calls=%async_computation.2 | async-start | bytes 131072 | tf_op jit(solution)/shard_map/all_to_all | solution.py:308
  40.3 4.2 %update.3 = (f32[2,512,1024]{2,1,0:T(8,128)}, f32[8,128]{1,0:T(8,128)}) custom-call(s32[1]{0:T(128)} %bitcast.base, f32[16,8,128]{2,1,0:T(8,128)} %copy-done.1, f32[8,1,128]{2,1,0:T(1,128)} %decay.1.decay_ref, f32[2,512,1024]{2,1,0:T(8,128)} %state_ref.5, bf16[16,16,128]{2,1,0:T(8,128)(2,1)} %read.1.rest_0_), custom_call_target="tpu_custom_call" | custom-call | flops 4194304 | bytes 4194304 | tf_op jit(solution)/shard_map/update/pallas_call | solution.py:410
  44.5 2.7 %all-to-all-done.2.got = bf16[16,16,128]{2,1,0:T(8,128)(2,1)S(1)} async-done(((bf16[16,16,128]{2,1,0:T(8,128)(2,1)}), bf16[16,16,128]{2,1,0:T(8,128)(2,1)S(1)}, u32[]{:S(2)}, u32[]{:S(2)}) %all-to-all-start.2) | async-done | bytes 65568 | tf_op jit(solution)/shard_map/all_to_all | solution.py:308
  47.8 2.7 %branch.1 = (bf16[8,256]{1,0:T(8,128)(2,1)}, bf16[16,8,256]{2,1,0:T(8,128)(2,1)}) custom-call(bf16[16,16,128]{2,1,0:T(8,128)(2,1)} %copy-done.4, bf16[8,256]{1,0:T(8,128)(2,1)} %res.1, bf16[4096,256]{1,0:T(8,128)(2,1)} %w.1, f32[8,128]{1,0:T(8,128)} %get-tuple-element.13.flag), custom_call_target="tpu_custom_call" | custom-call | flops 2097152 | bytes 2097152 | tf_op jit(solution)/shard_map/branch/pallas_call | solution.py:425
  50.5 3.5 %all-to-all-start.3 = ((bf16[16,8,256]{2,1,0:T(8,128)(2,1)}), bf16[16,8,256]{2,1,0:T(8,128)(2,1)S(1)}, u32[]{:S(2)}, u32[]{:S(2)}) async-start(bf16[16,8,256]{2,1,0:T(8,128)(2,1)} %get-tuple-element.15.rest_0_), calls=%async_computation.3 | async-start | bytes 131072 | tf_op jit(solution)/shard_map/all_to_all | solution.py:308
  54.0 2.3 %update.4 = (f32[2,512,1024]{2,1,0:T(8,128)}, f32[8,128]{1,0:T(8,128)}) custom-call(s32[1]{0:T(128)} %bitcast.base, f32[16,8,128]{2,1,0:T(8,128)} %copy-done.1, f32[8,1,128]{2,1,0:T(1,128)} %decay.1.decay_ref, f32[2,512,1024]{2,1,0:T(8,128)} %state_ref.5, bf16[16,8,256]{2,1,0:T(8,128)(2,1)} %get-tuple-element.15.rest_0_, ...), custom_call_target="tpu_custom_call", output_to_operand_aliasing={{0}: (5, {})} | custom-call | flops 2097152 | bytes 2097152 | tf_op jit(solution)/shard_map/update/pallas_call | solution.py:410
  56.4 4.5 %all-to-all-done.3.blocks = bf16[16,8,256]{2,1,0:T(8,128)(2,1)S(1)} async-done(((bf16[16,8,256]{2,1,0:T(8,128)(2,1)}), bf16[16,8,256]{2,1,0:T(8,128)(2,1)S(1)}, u32[]{:S(2)}, u32[]{:S(2)}) %all-to-all-start.3) | async-done | bytes 65568 | tf_op jit(solution)/shard_map/all_to_all | solution.py:308
  61.5 6.0 %expert.1.rest_0_ = bf16[16,8,256]{2,1,0:T(8,128)(2,1)} custom-call(bf16[16,8,256]{2,1,0:T(8,128)(2,1)} %copy-done.3, bf16[1,4096]{1,0:T(2,128)(2,1)} %broadcast_in_dim.37._gain.gain, f32[8,1]{1,0:T(8,128)} %copy.23._share.share, bf16[1,4096,512]{2,1,0:T(8,128)(2,1)} %wg.3, bf16[1,4096,512]{2,1,0:T(8,128)(2,1)} %wu.1, bf16[1,512,4096]{2,1,0:T(8,128)(2,1)} %wd.1, ...), custom_call_target="tpu_custom_call" | custom-call | flops 12582912 | bytes 12582912 | tf_op jit(solution)/shard_map/expert/pallas_call | solution.py:444
  67.6 3.5 %all-to-all-start.4 = ((bf16[16,8,256]{2,1,0:T(8,128)(2,1)}), bf16[16,8,256]{2,1,0:T(8,128)(2,1)S(1)}, u32[]{:S(2)}, u32[]{:S(2)}) async-start(bf16[16,8,256]{2,1,0:T(8,128)(2,1)} %expert.1.rest_0_), calls=%async_computation.4 | async-start | bytes 131072 | tf_op jit(solution)/shard_map/all_to_all | solution.py:308
  71.1 2.3 %update.5 = (f32[2,512,1024]{2,1,0:T(8,128)}, f32[8,128]{1,0:T(8,128)}) custom-call(s32[1]{0:T(128)} %bitcast.base, f32[16,8,128]{2,1,0:T(8,128)} %copy-done.1, f32[8,1,128]{2,1,0:T(1,128)} %decay.1.decay_ref, f32[2,512,1024]{2,1,0:T(8,128)} %state_ref.5, bf16[16,8,256]{2,1,0:T(8,128)(2,1)} %expert.1.rest_0_, ...), custom_call_target="tpu_custom_call", output_to_operand_aliasing={{0}: (5, {})} | custom-call | flops 2097152 | bytes 2097152 | tf_op jit(solution)/shard_map/update/pallas_call | solution.py:410
  73.4 4.5 %all-to-all-done.4 = bf16[16,8,256]{2,1,0:T(8,128)(2,1)S(1)} async-done(((bf16[16,8,256]{2,1,0:T(8,128)(2,1)}), bf16[16,8,256]{2,1,0:T(8,128)(2,1)S(1)}, u32[]{:S(2)}, u32[]{:S(2)}) %all-to-all-start.4) | async-done | bytes 65568 | tf_op jit(solution)/shard_map/all_to_all | solution.py:308
  (30 shorter events, 6.3 us)
Async XLA Ops:
  0.6 27.0 %copy-start = (bf16[16,2048]{1,0:T(8,128)(2,1)S(1)}, bf16[16,2048]{1,0:T(8,128)(2,1)}, u32[]{:S(2)}) copy-start(bf16[16,2048]{1,0:T(8,128)(2,1)} %param.27) | copy-start | bytes 196612
  0.6 24.5 %copy-start.9 = (s32[8,2]{0,1:T(2,128)S(1)}, s32[8,2]{0,1:T(2,128)}, u32[]{:S(2)}) copy-start(s32[8,2]{0,1:T(2,128)} %param.32) | copy-start | bytes 196
  0.7 24.5 %copy-start.10 = (f32[8,2]{0,1:T(2,128)S(1)}, f32[8,2]{0,1:T(2,128)}, u32[]{:S(2)}) copy-start(f32[8,2]{0,1:T(2,128)} %param.34) | copy-start | bytes 196
  0.7 25.2 %copy-start.7 = (bf16[1024]{0:T(1024)(128)(2,1)S(1)}, bf16[1024]{0:T(1024)(128)(2,1)}, u32[]{:S(2)}) copy-start(bf16[1024]{0:T(1024)(128)(2,1)} %param.29) | copy-start | bytes 6148
  0.7 25.7 %copy-start.5 = (bf16[4096]{0:T(1024)(128)(2,1)S(1)}, bf16[4096]{0:T(1024)(128)(2,1)}, u32[]{:S(2)}) copy-start(bf16[4096]{0:T(1024)(128)(2,1)} %param.31) | copy-start | bytes 24580
  0.7 26.4 %copy-start.8 = (f32[2048]{0:T(1024)S(1)}, f32[2048]{0:T(1024)}, u32[]{:S(2)}) copy-start(f32[2048]{0:T(1024)} %param.28) | copy-start | bytes 24580
  2.1 14.3 %all-to-all-start = ((bf16[16,8,256]{2,1,0:T(8,128)(2,1)}), bf16[16,8,256]{2,1,0:T(8,128)(2,1)S(1)}, u32[]{:S(2)}, u32[]{:S(2)}) async-start(bf16[16,8,256]{2,1,0:T(8,128)(2,1)} %broadcast_in_dim.33), calls=%async_computation | async-start | bytes 131072 | tf_op jit(solution)/shard_map/all_to_all | solution.py:308
  16.4 0.6 copy-start.2
  21.6 10.4 %all-to-all-start.1 = ((f32[16,8,128]{2,1,0:T(8,128)}), f32[16,8,128]{2,1,0:T(8,128)S(1)}, u32[]{:S(2)}, u32[]{:S(2)}) async-start(f32[16,8,128]{2,1,0:T(8,128)} %get-tuple-element.11), calls=%async_computation.1 | async-start | bytes 131072 | tf_op jit(solution)/shard_map/all_to_all | solution.py:308
  32.0 0.6 copy-start.1
  36.5 10.7 %all-to-all-start.2 = ((bf16[16,16,128]{2,1,0:T(8,128)(2,1)}), bf16[16,16,128]{2,1,0:T(8,128)(2,1)S(1)}, u32[]{:S(2)}, u32[]{:S(2)}) async-start(bf16[16,16,128]{2,1,0:T(8,128)(2,1)} %read.1.rest_0_), calls=%async_computation.2 | async-start | bytes 131072 | tf_op jit(solution)/shard_map/all_to_all | solution.py:308
  47.2 0.6 copy-start.4
  50.5 10.4 %all-to-all-start.3 = ((bf16[16,8,256]{2,1,0:T(8,128)(2,1)}), bf16[16,8,256]{2,1,0:T(8,128)(2,1)S(1)}, u32[]{:S(2)}, u32[]{:S(2)}) async-start(bf16[16,8,256]{2,1,0:T(8,128)(2,1)} %get-tuple-element.15.rest_0_), calls=%async_computation.3 | async-start | bytes 131072 | tf_op jit(solution)/shard_map/all_to_all | solution.py:308
  60.9 0.6 copy-start.3
  67.6 10.4 %all-to-all-start.4 = ((bf16[16,8,256]{2,1,0:T(8,128)(2,1)}), bf16[16,8,256]{2,1,0:T(8,128)(2,1)S(1)}, u32[]{:S(2)}, u32[]{:S(2)}) async-start(bf16[16,8,256]{2,1,0:T(8,128)(2,1)} %expert.1.rest_0_), calls=%async_computation.4 | async-start | bytes 131072 | tf_op jit(solution)/shard_map/all_to_all | solution.py:308
  71.1 6.9 %copy-start.6 = (bf16[8,256]{1,0:T(8,128)(2,1)S(1)}, bf16[8,256]{1,0:T(8,128)(2,1)}, u32[]{:S(2)}) copy-start(bf16[8,256]{1,0:T(8,128)(2,1)} %get-tuple-element.14) | copy-start | bytes 12292
